TPU v7x, 512 devices: a whole 4x4x16 slice. The times are simulated.
512 devices in a mesh: ep: 32 (over z, core), tp: 16 (over y, x).
Axes of the slice: x: 4, y: 4, z: 16, core: 2. Of those that a mesh axis runs over, the one named last changes fastest.
Arguments:
- query_rows: bfloat16 [24576, 1024], P('ep', 'tp'), may hold values from -600 to 600
- key_rows: bfloat16 [24576, 1024], P('ep', 'tp'), may hold values from -6 to 6
- value_rows: bfloat16 [24576, 1024], P('ep', 'tp'), may hold values from -6 to 6
- cum_gate: float32 [16, 24576], P('tp'), may hold values from -2458 to 0, as said below
- out_weight: bfloat16 [1024, 2048], P(None, 'tp'), may hold values from -0.1875 to 0.1875
- moe_input: bfloat16 [6144, 2048], P('ep'), may hold values from -6 to 6
- moe_gain: float32 [2048], replicated, may hold values from 0.1 to 1.9
- routes: int32 [6144, 3], P('ep'), may hold values from 0 to 127, all different within a row; in each aligned block of 192 rows (0 to 191, 192 to 383, ...) at most 9 rows name the same one
- route_weight: float32 [6144, 3], P('ep'), may hold values from 0.2 to 1.5
- expert_gate: bfloat16 [128, 2048, 512], P('ep', None, 'tp'), may hold values from -0.125 to 0.125
- expert_up: bfloat16 [128, 2048, 512], P('ep', None, 'tp'), may hold values from -0.125 to 0.125
- expert_down: bfloat16 [128, 512, 2048], P('ep', None, 'tp'), may hold values from -0.25 to 0.25
- shared_gate: bfloat16 [2048, 512], P(None, 'tp'), may hold values from -0.125 to 0.125
- shared_up: bfloat16 [2048, 512], P(None, 'tp'), may hold values from -0.125 to 0.125
- shared_down: bfloat16 [512, 2048], P(None, 'tp'), may hold values from -0.25 to 0.25
Outputs:
- mixer_out: bfloat16 [24576, 2048], P('ep', 'tp')
- moe_out: bfloat16 [6144, 2048], P('ep', 'tp')
Inputs may be any that keep to these rules, and one draw needn't show every extreme that they name: Non-increasing along positions: cum_gate[h, t] is the sum of the log forget gates of head h over positions 0 to t. `routes`: the 3 experts of a token differ. In each aligned block of 192 tokens no expert is named by more than 9 tokens, a bound that some block reaches.
All inputs are finite; a program needn't handle non-finite values.
Results may differ from a plain program's by a relative error of at most 0.0068.
Values may be sent and summed in bfloat16 or wider, within the bound.
No kernel may reach another device: no remote copies, remote signals or barrier semaphores. Data moves between devices by JAX's collectives and lax.ppermute only.
A program may use at most 64 MiB of HBM per device.

v0:
```python
import jax
import jax.numpy as jnp
from jax import lax
from jax.sharding import PartitionSpec as P

HEAD = 64
neg_fill = -1e30
norm_eps = 1e-06


def joined_along(pieces, dim):
    dims = list(pieces.shape[1:])
    dims[dim] *= pieces.shape[0]
    return jnp.moveaxis(pieces, 0, dim).reshape(dims)


def sent_to_all(array, axis):
    copies = jnp.broadcast_to(array, (lax.axis_size(axis), *array.shape))
    return lax.all_to_all(copies, axis, split_axis=0, concat_axis=0, tiled=True)


def collect(array, axis, dim):
    return joined_along(sent_to_all(array, axis), dim)


def local(
    query_rows,
    key_rows,
    value_rows,
    cum_gate,
    out_weight,
    moe_input,
    moe_gain,
    routes,
    route_weight,
    expert_gate,
    expert_up,
    expert_down,
    shared_gate,
    shared_up,
    shared_down,
):
    row_count = query_rows.shape[0]
    width = query_rows.shape[1]
    local_heads = width // HEAD
    scale = HEAD ** (-0.5)
    first_row = lax.axis_index("ep") * row_count
    last_row = first_row + row_count - 1
    query_heads = query_rows.reshape(row_count, local_heads, HEAD)
    query_gate = lax.dynamic_slice_in_dim(cum_gate, first_row, row_count, 1)
    query_pos = first_row + jnp.arange(row_count, dtype=jnp.int32)
    key_value = jnp.concatenate([key_rows, value_rows], axis=1)
    initial = (
        jnp.full((local_heads, row_count), neg_fill, jnp.float32),
        jnp.zeros((local_heads, row_count), jnp.float32),
        jnp.zeros((local_heads, row_count, HEAD), jnp.float32),
    )
    shard_rows = lax.all_gather(key_value, "ep", axis=0, tiled=True)
    piece_len = shard_rows.shape[0]
    key_span = 512

    def one_span(state_in, span_index):
        span_start = span_index * key_span

        def update(state_old):
            running_max, denominator, weighted = state_old
            block = lax.dynamic_slice_in_dim(shard_rows, span_index * key_span, key_span, 0)
            keys_block = block[:, :width].reshape(key_span, local_heads, HEAD)
            values_block = block[:, width:].reshape(key_span, local_heads, HEAD)
            key_gate = lax.dynamic_slice_in_dim(cum_gate, span_start, key_span, 1)
            scores = (
                jnp.einsum(
                    "qhd,khd->hqk", query_heads, keys_block, preferred_element_type=jnp.float32
                )
                * scale
            )
            scores = scores + query_gate[:, :, None] - key_gate[:, None, :]
            causal = (span_start + jnp.arange(key_span, dtype=jnp.int32))[None, :] <= query_pos[
                :, None
            ]
            scores = jnp.where(causal[None], scores, neg_fill)
            new_max = jnp.maximum(running_max, jnp.max(scores, axis=2))
            expon = jnp.where(causal[None], jnp.exp(scores - new_max[:, :, None]), 0.0)
            rescale = jnp.exp(running_max - new_max)
            denominator = denominator * rescale + jnp.sum(expon, axis=2)
            weighted = weighted * rescale[:, :, None] + jnp.einsum(
                "hqk,khd->hqd",
                expon.astype(jnp.bfloat16),
                values_block,
                preferred_element_type=jnp.float32,
            )
            return (new_max, denominator, weighted)

        state_next = lax.cond(span_start <= last_row, update, lambda unchanged: unchanged, state_in)
        return (state_next, None)

    state_out, _ = lax.scan(one_span, initial, jnp.arange(piece_len // key_span, dtype=jnp.int32))
    running_max, denominator, weighted = state_out
    heads_out = (weighted / denominator[:, :, None]).transpose(1, 0, 2).reshape(row_count, width)
    heads_out = heads_out.astype(jnp.bfloat16)
    token_count = moe_input.shape[0]
    top_count = routes.shape[1]
    local_experts = expert_gate.shape[0]
    ep_count = lax.axis_size("ep")
    expert_count = local_experts * ep_count
    capacity = 2 * token_count * top_count // expert_count
    column_count = expert_down.shape[2]
    first_column = lax.axis_index("tp") * column_count
    moe_rows = moe_input.astype(jnp.float32)
    normed = (
        moe_rows
        * lax.rsqrt(jnp.mean(moe_rows * moe_rows, axis=1, keepdims=True) + norm_eps)
        * moe_gain
    ).astype(jnp.bfloat16)
    flat_routes = routes.reshape(-1)
    one_hot = (flat_routes[:, None] == jnp.arange(expert_count, dtype=jnp.int32)[None, :]).astype(
        jnp.int32
    )
    ranks = jnp.sum(jnp.cumsum(one_hot, axis=0) * one_hot, axis=1) - 1
    slot_index = flat_routes * capacity + ranks
    pair_token = jnp.arange(token_count * top_count, dtype=jnp.int32) // top_count
    slot_token = (
        jnp.full((expert_count * capacity,), token_count, jnp.int32).at[slot_index].set(pair_token)
    )
    padded = jnp.concatenate([normed, jnp.zeros((1, normed.shape[1]), jnp.bfloat16)], axis=0)
    outgoing = lax.dynamic_slice_in_dim(padded, first_column, column_count, 1)[slot_token]
    outgoing = outgoing.reshape(ep_count, local_experts, capacity, outgoing.shape[1])
    arrived = lax.all_to_all(outgoing, "ep", split_axis=0, concat_axis=0, tiled=True)
    arrived = lax.all_gather(arrived, "tp", axis=3, tiled=True)
    gate_val = jnp.einsum(
        "aecd,edf->aecf", arrived, expert_gate, preferred_element_type=jnp.float32
    )
    up_val = jnp.einsum("aecd,edf->aecf", arrived, expert_up, preferred_element_type=jnp.float32)
    hidden = (jax.nn.silu(gate_val) * up_val).astype(jnp.bfloat16)
    hidden = collect(hidden, "tp", 3)
    result = jnp.einsum(
        "aecf,efd->aecd", hidden, expert_down, preferred_element_type=jnp.float32
    ).astype(jnp.bfloat16)
    returned = lax.all_to_all(result, "ep", split_axis=0, concat_axis=0, tiled=True)
    picked = returned.reshape(expert_count * capacity, column_count)[slot_index]
    picked = picked.astype(jnp.float32).reshape(token_count, top_count, column_count)
    routed = jnp.sum(picked * route_weight[:, :, None], axis=1)
    shared_hidden = (
        jax.nn.silu(jnp.dot(normed, shared_gate, preferred_element_type=jnp.float32))
        * jnp.dot(normed, shared_up, preferred_element_type=jnp.float32)
    ).astype(jnp.bfloat16)
    mixer_sum = jnp.dot(
        lax.all_gather(heads_out, "tp", axis=1, tiled=True),
        out_weight,
        preferred_element_type=jnp.float32,
    )
    shared_all = lax.all_gather(shared_hidden, "tp", axis=1, tiled=True)
    moe_total = routed + jnp.dot(shared_all, shared_down, preferred_element_type=jnp.float32)
    return (mixer_sum.astype(jnp.bfloat16), moe_total.astype(jnp.bfloat16))


def solution(mesh):
    placed = (
        P("ep", "tp"),
        P("ep", "tp"),
        P("ep", "tp"),
        P("tp", None),
        P(None, "tp"),
        P("ep", None),
        P(),
        P("ep", None),
        P("ep", None),
        P("ep", None, "tp"),
        P("ep", None, "tp"),
        P("ep", None, "tp"),
        P(None, "tp"),
        P(None, "tp"),
        P(None, "tp"),
    )
    return jax.shard_map(
        local, mesh=mesh, in_specs=placed, out_specs=(P("ep", "tp"), P("ep", "tp")), check_vma=False
    )
```

profile of v0, /device:TPU:1, one launch (start us, length us, event | category | flops | bytes accessed | tf_op | source)
XLA Modules:
  0.0 554.8 jit_solution(1330439696241112962)
XLA Ops:
  11.6 4.1 scatter_custom_fusion
  16.0 2.9 gather_fusion
  19.3 40.2 %all_to_all.15 = bf16[32,4,9,128]{3,1,2,0:T(4,128)(2,1)S(1)} all-to-all(bf16[32,4,9,128]{3,1,2,0:T(4,128)(2,1)S(1)} %copy.46), channel_id=1, replica_groups=mesh['ep'=32,'tp'=16] {'ep'}, dimensions={0} | all-to-all | bytes 589824 | tf_op jit(solution)/shard_map/all_to_all | solution.py:128
  61.6 63.6 %all-gather.7.cloned.1.call-done = bf16[32,4,9,2048]{3,0,2,1:T(8,128)(2,1)} async-done(((bf16[32,4,9,128]{3,0,2,1:T(8,128)(2,1)}), bf16[32,4,9,2048]{3,0,2,1:T(8,128)(2,1)}) %all-gather.7.cloned.1.call-update) | async-done | bytes 4718608 | tf_op jit(solution)/shard_map/all_gather | solution.py:129
  125.2 3.8 convolution_bitcast_fusion.2
  130.5 3.2 broadcast_bitcast_fusion
  133.7 7.8 %reshape.164 = bf16[16,2,18432]{2,1,0:T(2,128)(2,1)} reshape(bf16[16,4,9,32,32]{4,3,2,1,0:T(8,128)(2,1)} %broadcast_bitcast_fusion) | data formatting | bytes 2359296
  141.5 4.8 all-to-all-start.1
  147.2 58.1 %all-gather.5.cloned.1.call-done = bf16[24576,128]{1,0:T(8,128)(2,1)} async-done(((bf16[768,128]{1,0:T(8,128)(2,1)}), bf16[24576,128]{1,0:T(8,128)(2,1)}) %all-gather.5.cloned.1.call-update) | async-done | bytes 6291472 | tf_op jit(solution)/shard_map/all_gather | solution.py:58
  205.4 76.2 %while.15 = (s32[]{:T(128)}, f32[1,768]{1,0:T(1,128)S(1)}, f32[1,768]{1,0:T(1,128)S(1)}, f32[1,768,64]{1,2,0:T(8,128)S(1)}, s32[48]{0:T(128)S(1)}, /*index=5*/s3...) while((s32[]{:T(128)}, f32[1,768]{1,0:T(1,128)S(1)}, ...), condition=%wide.region_5.6_spmd.clone, body=%wide.region_0.5_spmd.clone.sunk | while | flops 106270224 | bytes 5566899 | solution.py:97
  206.7 4.7 conditional.3
  209.6 1.4 fusion.4
  212.6 4.7 conditional.3
  215.5 1.4 fusion.4
  218.6 4.7 conditional.3
  282.3 3.8 reshape.165
  286.1 3.1 bitcast_bitcast_fusion
  289.2 7.6 %copy.48 = bf16[32,4,9,16,32]{4,3,0,2,1:T(8,128)(2,1)} copy(bf16[32,4,9,16,32]{4,0,2,1,3:T(8,128)(2,1)S(1)} %bitcast_bitcast_fusion) | data formatting | bytes 2359296 | tf_op jit(solution)/shard_map/transpose | solution.py:14
  296.8 6.5 %reshape.124 = bf16[32,4,9,512]{3,0,2,1:T(8,128)(2,1)S(1)} reshape(bf16[32,4,9,16,32]{4,3,0,2,1:T(8,128)(2,1)} %copy.48) | data formatting | bytes 2359296 | tf_op jit(solution)/shard_map/reshape | solution.py:14
  304.7 213.7 %all-to-all-start.2 = ((bf16[32,4,9,128]{3,1,2,0:T(4,128)(2,1)}), bf16[32,4,9,128]{3,1,2,0:T(4,128)(2,1)S(1)}, u32[]{:S(2)}, u32[]{:S(2)}) async-start(bf16[32,4,9,128]{3,1,2,0:T(4,128)(2,1)} %copy.49), calls=%async_computation.2 | async-start | bytes 589824 | tf_op jit(solution)/shard_map/all_to_all | solution.py:139
  519.2 20.5 %all_gather.15 = bf16[192,512]{0,1:T(8,128)(2,1)S(1)} all-gather(bf16[192,32]{0,1:T(8,128)(2,1)S(1)} %fusion.27), channel_id=1, replica_groups=mesh['ep'=32,'tp'=16] {'tp'}, dimensions={1}, use_global_device_ids=true | all-gather | bytes 208896 | tf_op jit(solution)/shard_map/all_gather | solution.py:152
  539.7 2.2 all-to-all-done.2
  542.2 1.9 gather_fusion.1
  545.5 2.7 fusion.22
  (252 shorter events, 51.7 us)
Async XLA Ops:
  7.2 296.1 %copy-start = (bf16[4,512,128]{2,1,0:T(8,128)(2,1)S(1)}, bf16[4,512,128]{2,1,0:T(8,128)(2,1)}, u32[]{:S(2)}) copy-start(bf16[4,512,128]{2,1,0:T(8,128)(2,1)} %param.30) | copy-start | bytes 1572868
  7.2 118.0 %all-gather.7.cloned.1.call-start = ((), (), s32[]{:S(2)}) async-start(), calls=%async_computation.4 | async-start | bytes 5013504 | tf_op jit(solution)/shard_map/all_gather | solution.py:129
  10.9 4.8 copy-start.1
  10.9 4.8 copy-start.8
  19.0 41.4 %copy-start.6 = (bf16[768,64]{0,1:T(8,128)(2,1)S(1)}, bf16[768,64]{0,1:T(8,128)(2,1)}, u32[]{:S(2)}) copy-start(bf16[768,64]{0,1:T(8,128)(2,1)} %param.20) | copy-start | bytes 294916
  19.0 41.6 %copy-start.7 = (bf16[768,64]{0,1:T(8,128)(2,1)S(1)}, bf16[768,64]{0,1:T(8,128)(2,1)}, u32[]{:S(2)}) copy-start(bf16[768,64]{0,1:T(8,128)(2,1)} %param.21) | copy-start | bytes 294916
  19.3 105.9 %copy-start.11 = (bf16[4,2048,32]{1,2,0:T(8,128)(2,1)S(1)}, bf16[4,2048,32]{1,2,0:T(8,128)(2,1)}, u32[]{:S(2)}) copy-start(bf16[4,2048,32]{1,2,0:T(8,128)(2,1)} %param.28) | copy-start | bytes 1572868
  60.3 145.0 %all-gather.5.cloned.1.call-start = ((), (), s32[]{:S(2)}) async-start(), calls=%async_computation.3 | async-start | bytes 6488064 | tf_op jit(solution)/shard_map/all_gather | solution.py:58
  61.6 67.5 %copy-start.12 = (bf16[4,2048,32]{1,2,0:T(8,128)(2,1)S(1)}, bf16[4,2048,32]{1,2,0:T(8,128)(2,1)}, u32[]{:S(2)}) copy-start(bf16[4,2048,32]{1,2,0:T(8,128)(2,1)} %param.29) | copy-start | bytes 1572868
  125.2 3.9 copy-start.10
  141.5 63.9 %copy-start.13 = (bf16[768,64]{0,1:T(8,128)(2,1)S(1)}, bf16[768,64]{0,1:T(8,128)(2,1)}, u32[]{:S(2)}) copy-start(bf16[768,64]{0,1:T(8,128)(2,1)} %param.19) | copy-start | bytes 294916
  141.5 140.8 %all-to-all-start.1 = ((bf16[16,2,18432]{2,1,0:T(2,128)(2,1)}), bf16[16,2,18432]{2,1,0:T(2,128)(2,1)S(1)}, u32[]{:S(2)}, u32[]{:S(2)}) async-start(bf16[16,2,18432]{2,1,0:T(2,128)(2,1)} %reshape.164), calls=%async_computation.1 | async-start | bytes 2359296 | tf_op jit(solution)/shard_map/all_to_all | solution.py:19
  146.3 399.2 %all-gather.9.cloned.1.call-start = ((), (), s32[]{:S(2)}) async-start(), calls=%async_computation.5 | async-start | bytes 1671168 | tf_op jit(solution)/shard_map/all_gather | solution.py:148
  303.3 215.1 %copy-start.9 = (f32[192,3]{0,1:T(4,128)S(1)}, f32[192,3]{0,1:T(4,128)}, u32[]{:S(2)}) copy-start(f32[192,3]{0,1:T(4,128)} %param.27) | copy-start | bytes 6916
  303.3 215.2 %copy-start.4 = (bf16[2048,32]{0,1:T(8,128)(2,1)S(1)}, bf16[2048,32]{0,1:T(8,128)(2,1)}, u32[]{:S(2)}) copy-start(bf16[2048,32]{0,1:T(8,128)(2,1)} %param.31) | copy-start | bytes 393220
  303.8 215.1 %copy-start.5 = (bf16[2048,32]{0,1:T(8,128)(2,1)S(1)}, bf16[2048,32]{0,1:T(8,128)(2,1)}, u32[]{:S(2)}) copy-start(bf16[2048,32]{0,1:T(8,128)(2,1)} %param.32) | copy-start | bytes 393220
  304.7 237.3 %all-to-all-start.2 = ((bf16[32,4,9,128]{3,1,2,0:T(4,128)(2,1)}), bf16[32,4,9,128]{3,1,2,0:T(4,128)(2,1)S(1)}, u32[]{:S(2)}, u32[]{:S(2)}) async-start(bf16[32,4,9,128]{3,1,2,0:T(4,128)(2,1)} %copy.49), calls=%async_computation.2 | async-start | bytes 589824 | tf_op jit(solution)/shard_map/all_to_all | solution.py:139
  542.1 2.6 copy-start.3
  542.2 3.3 copy-start.2
Sparse Core Ops, SparseCore 0:
  60.4 64.7 all-gather.6
  127.9 77.4 all-gather.4
  282.4 260.1 all-gather.8
where the time goes:
time: 559 us; the launch traced here: 555 us
  starting transfers between devices  219 us (39%)
  waiting for transfers between devices  124 us (22%)
  local copies, waits for them, and re-layouts  76.5 us (14%)
  blocking collectives  60.7 us (11%)
  loops' own time  36.1 us (6%)
  matrix products  18.3 us (3%)
  between operations  14.2 us (3%)
  other arithmetic  6.13 us (1%)
    all_to_all x1, starting transfers between devices, local(): lax.all_to_all(result, 'ep', split_axis=0, concat_axis=0, tiled=True)  214 us
    all_gather x1, waiting for transfers between devices, local(): arrived = lax.all_gather(arrived, 'tp', axis=3, tiled=True)  63.6 us
    all_gather x1, waiting for transfers between devices, local(): shard_rows = lax.all_gather(key_value, 'ep', axis=0, tiled=True)  58.1 us
    all_to_all x1, blocking collectives, local(): lax.all_to_all(outgoing, 'ep', split_axis=0, concat_axis=0, tiled=True)  40.2 us
    another operation x1, loops' own time, local(): lax.scan(one_span, initial, jnp.arange(piece_len // key_span, dtype=jnp.i...  33.2 us
    dynamic_slice x48, local copies, waits for them, and re-layouts, local(): lax.scan(one_span, initial, jnp.arange(piece_len // key_span, dtype=jnp.i...  28.1 us
    all_gather x1, blocking collectives, local(): shared_all = lax.all_gather(shared_hidden, 'tp', axis=1, tiled=True)  20.5 us
    unnamed x35, local copies, waits for them, and re-layouts  16.1 us
  transfers between devices with their start and end apart: 5, of which 3 were waited for; matrix products, arithmetic and copies ran while one was open for 15% of the time, Pallas kernels for 0%

commit v1 on v0

--- a/solution.py
+++ b/solution.py
@@ -1,3 +1,4 @@
+import functools
 import jax
 import jax.numpy as jnp
 from jax import lax
@@ -6,6 +7,16 @@
 HEAD = 64
 neg_fill = -1e30
 norm_eps = 1e-06
+
+
+def things_perform(tile_in, a_name, d_out):
+    return jnp.concatenate(
+        lax.all_to_all(jnp.stack([tile_in for _ in range(lax.axis_size(a_name))]), a_name, 0, 0),
+        axis=d_out,
+    )
+
+
+run_modes_now = functools.partial(things_perform, a_name="tp", d_out=3)
 
 
 def joined_along(pieces, dim):
@@ -126,7 +137,7 @@
     outgoing = lax.dynamic_slice_in_dim(padded, first_column, column_count, 1)[slot_token]
     outgoing = outgoing.reshape(ep_count, local_experts, capacity, outgoing.shape[1])
     arrived = lax.all_to_all(outgoing, "ep", split_axis=0, concat_axis=0, tiled=True)
-    arrived = lax.all_gather(arrived, "tp", axis=3, tiled=True)
+    arrived = run_modes_now(arrived)
     gate_val = jnp.einsum(
         "aecd,edf->aecf", arrived, expert_gate, preferred_element_type=jnp.float32
     )

time: 559 us -> 494 us (0.88)
  waiting for transfers between devices: 124 us -> 2.22 us
  blocking collectives: 60.7 us -> 126 us
  starting transfers between devices: 219 us -> 212 us
    all_gather x1 -> x0, waiting for transfers between devices: 63.6 us -> none  [local(): arrived = lax.all_gather(arrived, 'tp', axis=3, tiled=True)]
    all_to_all x0 -> x1, blocking collectives: none -> 63.3 us  [things_perform(): lax.all_to_all(jnp.stack([tile_in for _ in range(lax.axis_size(a_name))])...]
    all_gather x1, waiting for transfers between devices: 58.1 us -> 0.01 us  [local(): shard_rows = lax.all_gather(key_value, 'ep', axis=0, tiled=True)]
    all_to_all x1, starting transfers between devices: 214 us -> 208 us  [local(): lax.all_to_all(result, 'ep', split_axis=0, concat_axis=0, tiled=True)]
    unnamed x35 -> x29, local copies, waits for them, and re-layouts: 16.1 us -> 18 us
  transfers between devices with their start and end apart: 5 -> 4, of which waited for: 3 -> 1; matrix products, arithmetic and copies ran while one was open for 15% -> 19% of each run, Pallas kernels for 0% -> 0%
where the time goes in v1:
time: 494 us; the launch traced here: 490 us
  starting transfers between devices  212 us (43%)
  blocking collectives  126 us (26%)
  local copies, waits for them, and re-layouts  78.5 us (16%)
  loops' own time  36.1 us (7%)
  matrix products  15.8 us (3%)
  between operations  14.5 us (3%)
  other arithmetic  4.95 us (1%)
    all_to_all x1, starting transfers between devices, local(): lax.all_to_all(result, 'ep', split_axis=0, concat_axis=0, tiled=True)  208 us
    all_to_all x1, blocking collectives, things_perform(): lax.all_to_all(jnp.stack([tile_in for _ in range(lax.axis_size(a_name))])...  63.3 us
    all_to_all x1, blocking collectives, local(): lax.all_to_all(outgoing, 'ep', split_axis=0, concat_axis=0, tiled=True)  41.7 us
    another operation x1, loops' own time, local(): lax.scan(one_span, initial, jnp.arange(piece_len // key_span, dtype=jnp.i...  33.2 us
    dynamic_slice x48, local copies, waits for them, and re-layouts, local(): lax.scan(one_span, initial, jnp.arange(piece_len // key_span, dtype=jnp.i...  28.1 us
    all_gather x1, blocking collectives, local(): shared_all = lax.all_gather(shared_hidden, 'tp', axis=1, tiled=True)  20.5 us
    unnamed x29, local copies, waits for them, and re-layouts  18 us
    transpose x2, local copies, waits for them, and re-layouts, joined_along(): return jnp.moveaxis(pieces, 0, dim).reshape(dims)  10.7 us
  transfers between devices with their start and end apart: 4, of which 1 were waited for; matrix products, arithmetic and copies ran while one was open for 19% of the time, Pallas kernels for 0%

profile of v1, /device:TPU:1, one launch (start us, length us, event | category | flops | bytes accessed | tf_op | source)
XLA Modules:
  0.0 489.6 jit_solution(5181445701204837118)
XLA Ops:
  13.2 4.1 scatter_custom_fusion
  17.9 2.9 gather_fusion
  21.1 41.7 %all_to_all.20 = bf16[32,4,9,128]{3,1,2,0:T(4,128)(2,1)S(1)} all-to-all(bf16[32,4,9,128]{3,1,2,0:T(4,128)(2,1)S(1)} %copy.49), channel_id=1, replica_groups=mesh['ep'=32,'tp'=16] {'ep'}, dimensions={0} | all-to-all | bytes 589824 | tf_op jit(solution)/shard_map/all_to_all | solution.py:139
  63.8 63.3 %all_to_all.21 = bf16[16,32,4,9,128]{4,1,3,2,0:T(8,128)(2,1)S(1)} all-to-all(bf16[16,32,4,9,128]{4,1,3,2,0:T(8,128)(2,1)S(1)} %stack.2), channel_id=1, replica_groups=mesh['ep'=32,'tp'=16] {'tp'}, dimensions={0} | all-to-all | bytes 9437184 | tf_op jit(solution)/shard_map/all_to_all | solution.py:14
  129.9 3.2 broadcast_bitcast_fusion
  133.1 7.8 %reshape.174 = bf16[16,2,18432]{2,1,0:T(2,128)(2,1)} reshape(bf16[16,4,9,32,32]{4,3,2,1,0:T(8,128)(2,1)} %broadcast_bitcast_fusion) | data formatting | bytes 2359296
  140.9 3.8 all-to-all-start.2
  145.7 76.2 %while.15 = (s32[]{:T(128)}, f32[1,768]{1,0:T(1,128)S(1)}, f32[1,768]{1,0:T(1,128)S(1)}, f32[1,768,64]{1,2,0:T(8,128)S(1)}, s32[48]{0:T(128)S(1)}, /*index=5*/s3...) while((s32[]{:T(128)}, f32[1,768]{1,0:T(1,128)S(1)}, ...), condition=%wide.region_5.6_spmd.clone, body=%wide.region_0.5_spmd.clone.sunk | while | flops 106270224 | bytes 5566899 | solution.py:108
  147.0 4.7 conditional.3
  148.5 1.4 fusion.56
  149.9 1.4 fusion.4
  153.0 4.7 conditional.3
  155.9 1.4 fusion.4
  158.9 4.7 conditional.3
  161.8 1.4 fusion.4
  222.7 3.8 reshape.175
  226.4 3.1 bitcast_bitcast_fusion
  229.6 7.6 %copy.52 = bf16[32,4,9,16,32]{4,3,0,2,1:T(8,128)(2,1)} copy(bf16[32,4,9,16,32]{4,0,2,1,3:T(8,128)(2,1)S(1)} %bitcast_bitcast_fusion) | data formatting | bytes 2359296 | tf_op jit(solution)/shard_map/transpose | solution.py:25
  237.2 6.5 %reshape.134 = bf16[32,4,9,512]{3,0,2,1:T(8,128)(2,1)S(1)} reshape(bf16[32,4,9,16,32]{4,3,0,2,1:T(8,128)(2,1)} %copy.52) | data formatting | bytes 2359296 | tf_op jit(solution)/shard_map/reshape | solution.py:25
  245.0 207.8 %all-to-all-start.3 = ((bf16[32,4,9,128]{3,1,2,0:T(4,128)(2,1)}), bf16[32,4,9,128]{3,1,2,0:T(4,128)(2,1)S(1)}, u32[]{:S(2)}, u32[]{:S(2)}) async-start(bf16[32,4,9,128]{3,1,2,0:T(4,128)(2,1)} %copy.53), calls=%async_computation.3 | async-start | bytes 589824 | tf_op jit(solution)/shard_map/all_to_all | solution.py:150
  453.7 20.5 %all_gather.11 = bf16[192,512]{0,1:T(8,128)(2,1)S(1)} all-gather(bf16[192,32]{0,1:T(8,128)(2,1)S(1)} %fusion.43), channel_id=1, replica_groups=mesh['ep'=32,'tp'=16] {'tp'}, dimensions={1}, use_global_device_ids=true | all-gather | bytes 208896 | tf_op jit(solution)/shard_map/all_gather | solution.py:163
  474.3 2.2 all-to-all-done.3
  476.7 1.9 gather_fusion.1
  480.0 2.7 fusion.38
  (245 shorter events, 51.0 us)
Async XLA Ops:
  7.2 236.5 %copy-start = (bf16[4,512,128]{2,1,0:T(8,128)(2,1)S(1)}, bf16[4,512,128]{2,1,0:T(8,128)(2,1)}, u32[]{:S(2)}) copy-start(bf16[4,512,128]{2,1,0:T(8,128)(2,1)} %param.30) | copy-start | bytes 1572868
  7.2 138.5 %all-gather.4.cloned.1.call-start = ((), (), s32[]{:S(2)}) async-start(), calls=%async_computation.4 | async-start | bytes 6488064 | tf_op jit(solution)/shard_map/all_gather | solution.py:69
  12.5 4.8 copy-start.1
  12.7 4.9 copy-start.6
  63.8 63.3 %copy-start.8 = (bf16[4,2048,32]{1,2,0:T(8,128)(2,1)S(1)}, bf16[4,2048,32]{1,2,0:T(8,128)(2,1)}, u32[]{:S(2)}) copy-start(bf16[4,2048,32]{1,2,0:T(8,128)(2,1)} %param.28) | copy-start | bytes 1572868
  127.2 1.4 copy-start.9
  140.9 4.8 copy-start.10
  140.9 81.7 %all-to-all-start.2 = ((bf16[16,2,18432]{2,1,0:T(2,128)(2,1)}), bf16[16,2,18432]{2,1,0:T(2,128)(2,1)S(1)}, u32[]{:S(2)}, u32[]{:S(2)}) async-start(bf16[16,2,18432]{2,1,0:T(2,128)(2,1)} %reshape.174), calls=%async_computation.2 | async-start | bytes 2359296 | tf_op jit(solution)/shard_map/all_to_all | solution.py:30
  144.8 335.2 %all-gather.6.cloned.1.call-start = ((), (), s32[]{:S(2)}) async-start(), calls=%async_computation.5 | async-start | bytes 1671168 | tf_op jit(solution)/shard_map/all_gather | solution.py:159
  243.6 209.2 %copy-start.7 = (f32[192,3]{0,1:T(4,128)S(1)}, f32[192,3]{0,1:T(4,128)}, u32[]{:S(2)}) copy-start(f32[192,3]{0,1:T(4,128)} %param.27) | copy-start | bytes 6916
  243.7 209.3 %copy-start.4 = (bf16[2048,32]{0,1:T(8,128)(2,1)S(1)}, bf16[2048,32]{0,1:T(8,128)(2,1)}, u32[]{:S(2)}) copy-start(bf16[2048,32]{0,1:T(8,128)(2,1)} %param.31) | copy-start | bytes 393220
  244.2 209.2 %copy-start.5 = (bf16[2048,32]{0,1:T(8,128)(2,1)S(1)}, bf16[2048,32]{0,1:T(8,128)(2,1)}, u32[]{:S(2)}) copy-start(bf16[2048,32]{0,1:T(8,128)(2,1)} %param.32) | copy-start | bytes 393220
  245.0 231.4 %all-to-all-start.3 = ((bf16[32,4,9,128]{3,1,2,0:T(4,128)(2,1)}), bf16[32,4,9,128]{3,1,2,0:T(4,128)(2,1)S(1)}, u32[]{:S(2)}, u32[]{:S(2)}) async-start(bf16[32,4,9,128]{3,1,2,0:T(4,128)(2,1)} %copy.53), calls=%async_computation.3 | async-start | bytes 589824 | tf_op jit(solution)/shard_map/all_to_all | solution.py:150
  476.6 2.6 copy-start.3
  476.7 3.3 copy-start.2
Sparse Core Ops, SparseCore 0:
  10.7 92.6 all-gather.3
  222.8 254.3 all-gather.5
